TPU v7x, 32 devices: a whole 2x2x4 slice. The times are simulated.
32 devices in a mesh: sp: 16 (over z, y, x), tp: 2 (over core).
Axes of the slice: x: 2, y: 2, z: 4, core: 2. Of those that a mesh axis runs over, the one named last changes fastest.
Arguments:
- query_one: bfloat16 [2048, 1024], P('sp', 'tp'), may hold values from -6 to 6
- key_one: bfloat16 [2048, 1024], P('sp', 'tp'), may hold values from -6 to 6
- query_two: bfloat16 [2048, 512], P('sp', 'tp'), may hold values from -6 to 6
- key_two: bfloat16 [2048, 512], P('sp', 'tp'), may hold values from -6 to 6
- values: bfloat16 [2048, 2048], P('sp', 'tp'), may hold values from -6 to 6
- out_gate: bfloat16 [2048, 2048], P('sp', 'tp'), may hold values from -6 to 6
- in_gate: float32 [16, 2048], P('tp', 'sp'), may hold values from -3 to 150
- forget_gate: float32 [16, 2048], P('tp', 'sp'), may hold values from -1 to 24
- head_gain: float32 [2048], P('tp'), may hold values from 0.1 to 1.9
- out_weight: bfloat16 [2048, 2048], P('tp'), may hold values from -0.125 to 0.125
- stream: bfloat16 [2048, 2048], P('sp'), may hold values from -6 to 6
- mix_gain: float32 [2048], replicated, may hold values from 0.1 to 1.9
- up_weight: bfloat16 [2048, 8192], P('sp', 'tp'), may hold values from -0.125 to 0.125
- down_weight: bfloat16 [8192, 2048], P('tp', 'sp'), may hold values from -0.0625 to 0.0625
- out_gain: float32 [2048], replicated, may hold values from 0.1 to 1.9
Outputs:
- result: bfloat16 [2048, 2048], P(('sp', 'tp'))
All inputs are finite; a program needn't handle non-finite values.
Results may differ from a plain program's by a relative error of at most 0.018.
Values may be sent and summed in bfloat16 or wider, within the bound.
A program may use at most 128 MiB of HBM per device.

v0:
```python
from functools import partial
import jax
import jax.numpy as jnp
from jax import lax
from jax.sharding import PartitionSpec as P

BLOCK = 64
NEG_BIG = -1e30
EPS = 1e-05


def prefix_2(part, axis, combine, identity):
    place = lax.axis_index(axis)
    gathered = jax.tree.map(lambda a: lax.all_gather(a, axis), part)
    state = jax.tree.map(lambda a, e: jnp.zeros_like(a) + jnp.asarray(e, a.dtype), part, identity)

    def one(lap, state):
        return combine(
            state, jax.tree.map(lambda a: lax.dynamic_index_in_dim(a, lap, 0, False), gathered)
        )

    return lax.fori_loop(0, place, one, state)


def combine(earlier, later):
    decay_early, cell_early, norm_early, peak_early = earlier
    decay_late, cell_late, norm_late, peak_late = later
    ceiling = jnp.maximum(decay_late + peak_early, peak_late)
    keep_share = jnp.exp(decay_late + peak_early - ceiling)
    fresh_share = jnp.exp(peak_late - ceiling)
    cell_new = keep_share[..., None, None] * cell_early + fresh_share[..., None, None] * cell_late
    norm_new = keep_share[..., None] * norm_early + fresh_share[..., None] * norm_late
    return (decay_early + decay_late, cell_new, norm_new, ceiling)


def combine_groups(earlier, later):
    return (combine(earlier[0], later[0]), combine(earlier[1], later[1]))


def summarize(queries, keys_in, values_in, in_pre, forget_pre, block_len):
    length, width_k = queries.shape
    block_count = length // block_len
    scaled_keys = keys_in.astype(jnp.float32).reshape(
        block_count, block_len, width_k
    ) * width_k ** (-0.5)
    values_f = values_in.astype(jnp.float32).reshape(block_count, block_len, -1)
    width_v = values_f.shape[-1]
    log_forget = jax.nn.log_sigmoid(forget_pre).reshape(block_count, block_len)
    log_input = in_pre.reshape(block_count, block_len)
    cumulative = jnp.cumsum(log_forget, 1)
    decay_total = cumulative[:, -1]
    weight_log = decay_total[:, None] - cumulative + log_input
    peak_log = jnp.max(weight_log, 1)
    weighted = jnp.exp(weight_log - peak_log[:, None])[..., None] * scaled_keys
    cell_states = jnp.einsum("cld,cle->cde", weighted, values_f, precision=lax.Precision.HIGHEST)
    norm_states = jnp.sum(weighted, 1)
    identity = (
        jnp.zeros((), jnp.float32),
        jnp.zeros((width_k, width_v), jnp.float32),
        jnp.zeros((width_k,), jnp.float32),
        jnp.full((), NEG_BIG, jnp.float32),
    )

    def advance(running, element):
        return (combine(running, element), running)

    closing, prefix = lax.scan(advance, identity, (decay_total, cell_states, norm_states, peak_log))
    return (closing, prefix, (scaled_keys, values_f, cumulative, log_input))


def finish(queries, prefix, pieces, incoming):
    scaled_keys, values_f, cumulative, log_input = pieces
    block_count, block_len, width_k = scaled_keys.shape
    spread_in = jax.tree.map(
        lambda leaf: jnp.broadcast_to(leaf, (block_count,) + leaf.shape), incoming
    )
    _, cell_states, norm_states, peaks = combine(spread_in, prefix)
    query_f = queries.astype(jnp.float32).reshape(block_count, block_len, width_k)
    log_gaps = cumulative[:, :, None] - cumulative[:, None, :] + log_input[:, None, :]
    causal = jnp.arange(block_len)[:, None] >= jnp.arange(block_len)[None, :]
    log_gaps = jnp.where(causal[None], log_gaps, -jnp.inf)
    carried = cumulative + peaks[:, None]
    ceiling = jnp.maximum(carried, jnp.max(log_gaps, 2))
    scores = jnp.einsum("cld,csd->cls", query_f, scaled_keys, precision=lax.Precision.HIGHEST)
    scores = scores * jnp.exp(log_gaps - ceiling[..., None])
    carry_weight = jnp.exp(carried - ceiling)
    numerator = carry_weight[..., None] * jnp.einsum(
        "cld,cde->cle", query_f, cell_states, precision=lax.Precision.HIGHEST
    )
    numerator = numerator + jnp.einsum(
        "cls,cse->cle", scores, values_f, precision=lax.Precision.HIGHEST
    )
    denominator = carry_weight * jnp.einsum(
        "cld,cd->cl", query_f, norm_states, precision=lax.Precision.HIGHEST
    )
    denominator = denominator + jnp.sum(scores, 2)
    result = numerator / jnp.maximum(jnp.abs(denominator), jnp.exp(-ceiling))[..., None]
    return result.reshape(block_count * block_len, -1)


def head_norm(cell_out):
    center = jnp.mean(cell_out, -1, keepdims=True)
    spread = jnp.mean(jnp.square(cell_out - center), -1, keepdims=True)
    return (cell_out - center) * lax.rsqrt(spread + EPS)


def layer_norm(rows_f, gain):
    center = jnp.mean(rows_f, -1, keepdims=True)
    spread = jnp.mean(jnp.square(rows_f - center), -1, keepdims=True)
    return (rows_f - center) * lax.rsqrt(spread + EPS) * gain


def empty_state(head_pairs, width_k, width_v):
    return (
        jnp.zeros((head_pairs,), jnp.float32),
        jnp.zeros((head_pairs, width_k, width_v), jnp.float32),
        jnp.zeros((head_pairs, width_k), jnp.float32),
        jnp.full((head_pairs,), NEG_BIG, jnp.float32),
    )


def body(
    query_one,
    key_one,
    query_two,
    key_two,
    values,
    out_gate,
    in_gate,
    forget_gate,
    head_gain,
    out_weight,
    stream,
    mix_gain,
    up_weight,
    down_weight,
    out_gain,
):
    length = stream.shape[0]
    head_pairs = in_gate.shape[0] // 2
    width_v = values.shape[1] // (2 * head_pairs)

    def split_heads(array):
        return array.reshape(length, head_pairs, -1).transpose(1, 0, 2)

    values_split = values.reshape(length, head_pairs, 2, width_v).transpose(1, 2, 0, 3)
    input_rows = in_gate.reshape(head_pairs, 2, length)
    forget_rows = forget_gate.reshape(head_pairs, 2, length)
    summary = jax.vmap(partial(summarize, block_len=BLOCK))
    queries_one = split_heads(query_one)
    queries_two = split_heads(query_two)
    closing_one, prefix_one, pieces_one = summary(
        queries_one, split_heads(key_one), values_split[:, 0], input_rows[:, 0], forget_rows[:, 0]
    )
    closing_two, prefix_two, pieces_two = summary(
        queries_two, split_heads(key_two), values_split[:, 1], input_rows[:, 1], forget_rows[:, 1]
    )
    identity = (
        empty_state(head_pairs, queries_one.shape[2], width_v),
        empty_state(head_pairs, queries_two.shape[2], width_v),
    )
    incoming = prefix_2((closing_one, closing_two), "sp", combine_groups, identity)
    cell_one = jax.vmap(finish)(queries_one, prefix_one, pieces_one, incoming[0])
    cell_two = jax.vmap(finish)(queries_two, prefix_two, pieces_two, incoming[1])
    normed = jnp.stack([head_norm(cell_one), head_norm(cell_two)], 1)
    normed = normed.transpose(2, 0, 1, 3).reshape(length, 2 * head_pairs * width_v)
    mixed_heads = (normed * head_gain * jax.nn.sigmoid(out_gate.astype(jnp.float32))).astype(
        jnp.bfloat16
    )
    own_rows = length // lax.axis_size("tp")
    leading = lax.axis_index("tp") * own_rows
    up_full, down_full = (
        lax.all_gather(up_weight, "sp", axis=0, tiled=True),
        lax.all_gather(down_weight, "sp", axis=1, tiled=True),
    )
    summed = lax.psum_scatter(
        jnp.dot(mixed_heads, out_weight, preferred_element_type=jnp.float32).astype(jnp.bfloat16),
        "tp",
        scatter_dimension=0,
        tiled=True,
    )
    mixer_out = lax.optimization_barrier(summed)
    stream_own = lax.dynamic_slice_in_dim(stream, leading, own_rows, 0)
    first_own = layer_norm(
        stream_own.astype(jnp.float32) + mixer_out.astype(jnp.float32), mix_gain
    ).astype(jnp.bfloat16)
    hidden = jnp.square(
        jax.nn.relu(
            jnp.dot(
                lax.all_gather(first_own, "tp", axis=0, tiled=True),
                up_full,
                preferred_element_type=jnp.float32,
            )
        )
    ).astype(jnp.bfloat16)
    partial_sums = jnp.dot(hidden, down_full, preferred_element_type=jnp.float32)
    mlp_out = lax.optimization_barrier(
        lax.psum_scatter(partial_sums.astype(jnp.bfloat16), "tp", scatter_dimension=0, tiled=True)
    )
    return layer_norm(first_own.astype(jnp.float32) + mlp_out.astype(jnp.float32), out_gain).astype(
        jnp.bfloat16
    )


def solution(mesh):
    in_specs = (
        P("sp", "tp"),
        P("sp", "tp"),
        P("sp", "tp"),
        P("sp", "tp"),
        P("sp", "tp"),
        P("sp", "tp"),
        P("tp", "sp"),
        P("tp", "sp"),
        P("tp"),
        P("tp", None),
        P("sp", None),
        P(),
        P("sp", "tp"),
        P("tp", "sp"),
        P(),
    )
    out_specs = P(("sp", "tp"), None)
    return jax.shard_map(body, mesh=mesh, in_specs=in_specs, out_specs=out_specs, check_vma=False)
```

profile of v0, /device:TPU:0, one launch (start us, length us, event | category | flops | bytes accessed | tf_op | source)
XLA Modules:
  0.0 683.7 jit_solution(4655088481596444945)
XLA Ops:
  6.6 0.8 fusion.72
  7.5 1.0 reduce_window_sum.18
  8.7 0.8 fusion.88
  9.8 1.1 reshape.275
  11.0 1.0 copy.76
  12.7 0.7 while.76
  13.4 0.6 copy-done.1
  14.2 1.0 reduce_window_sum.17
  16.2 0.7 convolution_bitcast_fusion
  16.9 0.8 while.75
  17.7 0.7 copy-done
  18.6 0.6 dynamic-slice
  20.6 43.8 %all-reduce.4 = (f32[64]{0:T(128)S(1)}, f32[64]{0:T(128)S(1)}, f32[64]{0:T(128)S(1)}, f32[64]{0:T(128)S(1)}) all-reduce(f32[64]{0:T(128)S(1)} %dynamic-update-slice, f32[64]{0:T(128)S(1)} %dynamic-update-slice.1, f32[64]{0:T(128)S(1)} %dynamic-update-slice.2, f32[64]{0:T(128)S(1)} %dynamic-update-slice.3), channel_id=2, replica_groups=mesh['sp'=16,'tp'=2] {'sp'}, use_global_device_ids=true, to_apply=%add | all-reduce | flops 256 | bytes 2048
  65.1 36.1 %all-gather.9 = f32[16,4,64]{2,1,0:T(4,128)S(1)} all-gather(f32[1,4,64]{2,1,0:T(4,128)S(1)} %bitcast.311), channel_id=9, replica_groups=mesh['sp'=16,'tp'=2] {'sp'}, dimensions={0}, use_global_device_ids=true | all-gather | bytes 17408 | tf_op jit(solution)/shard_map/all_gather | solution.py:14
  101.3 37.9 %all-gather.8 = f32[16,4,128]{2,1,0:T(4,128)S(1)} all-gather(f32[1,4,128]{2,1,0:T(4,128)S(1)} %bitcast.312), channel_id=5, replica_groups=mesh['sp'=16,'tp'=2] {'sp'}, dimensions={0}, use_global_device_ids=true | all-gather | bytes 34816 | tf_op jit(solution)/shard_map/all_gather | solution.py:14
  139.6 15.4 %all-gather.19.cloned.1.call-done = f32[64,128,128]{2,1,0:T(8,128)} async-done(((f32[4,128,128]{2,1,0:T(8,128)}), f32[64,128,128]{2,1,0:T(8,128)}) %all-gather.19.cloned.1.call-update) | async-done | bytes 4194320 | tf_op jit(solution)/shard_map/all_gather | solution.py:14
  156.7 0.5 fusion.92
  161.0 3.8 convolution_convert_fusion.1
  164.9 0.5 all-gather.15.cloned.1.call-update
  165.5 0.5 all-gather.17.cloned.1.call-update
  166.1 39.8 %reduce-scatter.3.cloned.1.call-done = bf16[64,2048]{1,0:T(8,128)(2,1)} async-done(((bf16[128,2048]{1,0:T(8,128)(2,1)}), bf16[64,2048]{1,0:T(8,128)(2,1)}) %reduce-scatter.3.cloned.1.call-update) | async-done | bytes 262160 | tf_op jit(solution)/shard_map/reduce_scatter | solution.py:176
  206.0 1.1 fusion.39
  207.1 1.2 multiply_reduce_fusion.1
  208.3 1.1 multiply_convert_fusion.1
  209.4 2.4 all_gather.73
  211.8 189.0 %all-gather.15.cloned.1.call-done = bf16[2048,4096]{1,0:T(8,128)(2,1)} async-done(((bf16[128,4096]{1,0:T(8,128)(2,1)}), bf16[2048,4096]{1,0:T(8,128)(2,1)}) %all-gather.15.cloned.1.call-update) | async-done | bytes 16777232 | tf_op jit(solution)/shard_map/all_gather | solution.py:173
  400.7 249.9 %all-gather.17.cloned.1.call-done = bf16[4096,2048]{1,0:T(8,128)(2,1)} async-done(((bf16[4096,128]{1,0:T(8,128)(2,1)}), bf16[4096,2048]{1,0:T(8,128)(2,1)}) %all-gather.17.cloned.1.call-update) | async-done | bytes 16777232 | tf_op jit(solution)/shard_map/all_gather | solution.py:174
  650.6 15.9 %convolution_convert_fusion = bf16[128,2048]{1,0:T(8,128)(2,1)} fusion(bf16[4096,2048]{1,0:T(8,128)(2,1)} %all-gather.17.cloned.1.call-done, bf16[128,2048]{1,0:T(8,128)(2,1)S(1)} %all_gather.73, bf16[2048,4096]{1,0:T(8,128)(2,1)} %all-gather.15.cloned.1.call-done), kind=kOutput, calls=%fused_computation.65 | convolution fusion | flops 4296802304 | bytes 34603008 | tf_op jit(solution)/shard_map/dot_general | solution.py:196
  666.5 6.3 reduce-scatter.5.cloned.1.call-done
  672.8 1.1 fusion.41
  673.9 1.2 multiply_reduce_fusion
  675.1 1.8 multiply_convert_fusion
  (173 shorter events, 11.5 us)
Async XLA Ops:
  6.5 9.0 %copy-start.3 = (bf16[128,512]{1,0:T(8,128)(2,1)S(1)}, bf16[128,512]{1,0:T(8,128)(2,1)}, u32[]{:S(2)}) copy-start(bf16[128,512]{1,0:T(8,128)(2,1)} %param.22) | copy-start | bytes 393220
  6.5 133.0 %all-gather.21.cloned.1.call-start = ((), (), s32[]{:S(2)}) async-start(), calls=%async_computation.7 | async-start | bytes 2228224 | tf_op jit(solution)/shard_map/all_gather | solution.py:14
  13.4 0.6 copy-start.1
  14.0 140.9 %all-gather.19.cloned.1.call-start = ((), (), s32[]{:S(2)}) async-start(), calls=%async_computation.6 | async-start | bytes 4456448 | tf_op jit(solution)/shard_map/all_gather | solution.py:14
  16.2 2.4 copy-start.10
  16.2 48.6 %copy-start.4 = (bf16[128,512]{1,0:T(8,128)(2,1)S(1)}, bf16[128,512]{1,0:T(8,128)(2,1)}, u32[]{:S(2)}) copy-start(bf16[128,512]{1,0:T(8,128)(2,1)} %param.21) | copy-start | bytes 393220
  16.9 48.0 %copy-start.5 = (bf16[128,256]{1,0:T(8,128)(2,1)S(1)}, bf16[128,256]{1,0:T(8,128)(2,1)}, u32[]{:S(2)}) copy-start(bf16[128,256]{1,0:T(8,128)(2,1)} %param.23) | copy-start | bytes 196612
  17.7 0.7 copy-start
  18.4 187.6 %reduce-scatter.3.cloned.1.call-start = ((), (), s32[]{:S(2)}) async-start(), calls=%async_computation.2 | async-start | bytes 786432 | tf_op jit(solution)/shard_map/reduce_scatter | solution.py:176
  157.2 3.8 copy-start.8
  157.2 3.8 copy-start.9
  161.0 44.9 %copy-start.2 = (bf16[128,2048]{1,0:T(8,128)(2,1)S(1)}, bf16[128,2048]{1,0:T(8,128)(2,1)}, u32[]{:S(2)}) copy-start(bf16[128,2048]{1,0:T(8,128)(2,1)} %param.31) | copy-start | bytes 1572868
  161.0 47.3 %copy-start.6 = (f32[2048]{0:T(1024)S(1)}, f32[2048]{0:T(1024)}, u32[]{:S(2)}) copy-start(f32[2048]{0:T(1024)} %param.32) | copy-start | bytes 24580
  164.9 235.8 %all-gather.15.cloned.1.call-start = ((), (), s32[]{:S(2)}) async-start(), calls=%async_computation.3 | async-start | bytes 17825792 | tf_op jit(solution)/shard_map/all_gather | solution.py:173
  165.5 485.1 %all-gather.17.cloned.1.call-start = ((), (), s32[]{:S(2)}) async-start(), calls=%async_computation.4 | async-start | bytes 17825792 | tf_op jit(solution)/shard_map/all_gather | solution.py:174
  166.1 506.7 %reduce-scatter.5.cloned.1.call-start = ((), (), s32[]{:S(2)}) async-start(), calls=%async_computation.5 | async-start | bytes 786432 | tf_op jit(solution)/shard_map/reduce_scatter | solution.py:198
  211.8 463.3 %copy-start.7 = (f32[2048]{0:T(1024)S(1)}, f32[2048]{0:T(1024)}, u32[]{:S(2)}) copy-start(f32[2048]{0:T(1024)} %param.35) | copy-start | bytes 24580
Sparse Core Ops, SparseCore 0:
  14.2 63.5 all-gather.20
  80.5 74.4 all-gather.18
  165.0 40.8 reduce-scatter.2
  208.6 192.1 all-gather.14
  403.3 247.2 all-gather.16
  666.6 6.0 reduce-scatter.4
where the time goes:
time: 685 us; the launch traced here: 684 us
  waiting for transfers between devices  501 us (73%)
  blocking collectives  120 us (18%)
  matrix products  23.7 us (3%)
  between operations  14.6 us (2%)
  other arithmetic  13.8 us (2%)
  local copies, waits for them, and re-layouts  9.5 us (1%)
    all_gather x1, waiting for transfers between devices, body(): lax.all_gather(down_weight, 'sp', axis=1, tiled=True)  250 us
    all_gather x1, waiting for transfers between devices, body(): lax.all_gather(up_weight, 'sp', axis=0, tiled=True)  189 us
    all_gather x2, blocking collectives, prefix_2(): gathered = jax.tree.map(lambda a: lax.all_gather(a, axis), part)  74.1 us
    unnamed x1, blocking collectives  43.8 us
    reduce_scatter x1, waiting for transfers between devices, body(): lax.psum_scatter(jnp.dot(mixed_heads, out_weight, preferred_element_type=...  39.8 us
    dot_general x1, matrix products, body(): jnp.dot(hidden, down_full, preferred_element_type=jnp.float32)  15.9 us
    all_gather x2, waiting for transfers between devices, prefix_2(): gathered = jax.tree.map(lambda a: lax.all_gather(a, axis), part)  15.4 us
  transfers between devices with their start and end apart: 6, of which 5 were waited for; matrix products, arithmetic and copies ran while one was open for 1% of the time, Pallas kernels for 0%

commit v1 on v0

--- a/solution.py
+++ b/solution.py
@@ -7,6 +7,14 @@
 BLOCK = 64
 NEG_BIG = -1e30
 EPS = 1e-05
+
+
+def tiled_gather(shard, axis, dim):
+    size = lax.axis_size(axis)
+    repeats = [size if d == dim else 1 for d in range(shard.ndim)]
+    return lax.all_to_all(
+        jnp.tile(shard, repeats), axis, split_axis=dim, concat_axis=dim, tiled=True
+    )
 
 
 def prefix_2(part, axis, combine, identity):
@@ -170,7 +178,7 @@
     own_rows = length // lax.axis_size("tp")
     leading = lax.axis_index("tp") * own_rows
     up_full, down_full = (
-        lax.all_gather(up_weight, "sp", axis=0, tiled=True),
+        tiled_gather(up_weight, "sp", 0),
         lax.all_gather(down_weight, "sp", axis=1, tiled=True),
     )
     summed = lax.psum_scatter(

time: 685 us -> 828 us (1.21)
  waiting for transfers between devices: 501 us -> 600 us
  starting transfers between devices: 0.2 us -> 38.9 us
    all_to_all x0 -> x1, waiting for transfers between devices: none -> 368 us  [tiled_gather(): lax.all_to_all(jnp.tile(shard, repeats), axis, split_axis=dim, concat_axi...]
    all_gather x1 -> x0, waiting for transfers between devices: 189 us -> none  [body(): lax.all_gather(up_weight, 'sp', axis=0, tiled=True)]
    all_gather x1, waiting for transfers between devices: 250 us -> 192 us  [body(): lax.all_gather(down_weight, 'sp', axis=1, tiled=True)]
    reduce_scatter x1, waiting for transfers between devices: 39.8 us -> 0.02 us  [body(): lax.psum_scatter(jnp.dot(mixed_heads, out_weight, preferred_element_type=...]
    all_to_all x0 -> x1, starting transfers between devices: none -> 38.8 us  [tiled_gather(): lax.all_to_all(jnp.tile(shard, repeats), axis, split_axis=dim, concat_axi...]
    reduce_scatter x1, waiting for transfers between devices: 6.26 us -> 23.5 us  [body(): lax.psum_scatter(partial_sums.astype(jnp.bfloat16), 'tp', scatter_dimensi...]
  transfers between devices with their start and end apart: 6 -> 6, of which waited for: 5 -> 4; matrix products, arithmetic and copies ran while one was open for 1% -> 2% of each run, Pallas kernels for 0% -> 0%
where the time goes in v1:
time: 828 us; the launch traced here: 826 us
  waiting for transfers between devices  600 us (72%)
  blocking collectives  120 us (14%)
  starting transfers between devices  38.9 us (5%)
  matrix products  23.6 us (3%)
  local copies, waits for them, and re-layouts  15.4 us (2%)
  between operations  14.3 us (2%)
  other arithmetic  13.8 us (2%)
    all_to_all x1, waiting for transfers between devices, tiled_gather(): lax.all_to_all(jnp.tile(shard, repeats), axis, split_axis=dim, concat_axi...  368 us
    all_gather x1, waiting for transfers between devices, body(): lax.all_gather(down_weight, 'sp', axis=1, tiled=True)  192 us
    all_gather x2, blocking collectives, prefix_2(): gathered = jax.tree.map(lambda a: lax.all_gather(a, axis), part)  74.1 us
    unnamed x1, blocking collectives  43.8 us
    all_to_all x1, starting transfers between devices, tiled_gather(): lax.all_to_all(jnp.tile(shard, repeats), axis, split_axis=dim, concat_axi...  38.8 us
    reduce_scatter x1, waiting for transfers between devices, body(): lax.psum_scatter(partial_sums.astype(jnp.bfloat16), 'tp', scatter_dimensi...  23.5 us
  transfers between devices with their start and end apart: 6, of which 4 were waited for; matrix products, arithmetic and copies ran while one was open for 2% of the time, Pallas kernels for 0%

profile of v1, /device:TPU:0, one launch (start us, length us, event | category | flops | bytes accessed | tf_op | source)
XLA Modules:
  0.0 826.3 jit_solution(10255366027202259209)
XLA Ops:
  6.6 0.8 fusion.72
  7.5 1.0 reduce_window_sum.18
  8.7 0.8 fusion.88
  9.8 1.1 reshape.282
  11.0 1.0 copy.76
  12.7 0.7 while.76
  13.4 0.6 copy-done.1
  14.2 1.0 reduce_window_sum.17
  16.2 0.7 convolution_bitcast_fusion
  16.9 0.8 while.75
  17.7 0.7 copy-done
  18.6 0.6 dynamic-slice
  20.6 43.8 %all-reduce.4 = (f32[64]{0:T(128)S(1)}, f32[64]{0:T(128)S(1)}, f32[64]{0:T(128)S(1)}, f32[64]{0:T(128)S(1)}) all-reduce(f32[64]{0:T(128)S(1)} %dynamic-update-slice, f32[64]{0:T(128)S(1)} %dynamic-update-slice.1, f32[64]{0:T(128)S(1)} %dynamic-update-slice.2, f32[64]{0:T(128)S(1)} %dynamic-update-slice.3), channel_id=2, replica_groups=mesh['sp'=16,'tp'=2] {'sp'}, use_global_device_ids=true, to_apply=%add | all-reduce | flops 256 | bytes 2048
  65.1 36.1 %all-gather.9 = f32[16,4,64]{2,1,0:T(4,128)S(1)} all-gather(f32[1,4,64]{2,1,0:T(4,128)S(1)} %bitcast.312), channel_id=9, replica_groups=mesh['sp'=16,'tp'=2] {'sp'}, dimensions={0}, use_global_device_ids=true | all-gather | bytes 17408 | tf_op jit(solution)/shard_map/all_gather | solution.py:22
  101.3 37.9 %all-gather.8 = f32[16,4,128]{2,1,0:T(4,128)S(1)} all-gather(f32[1,4,128]{2,1,0:T(4,128)S(1)} %bitcast.313), channel_id=5, replica_groups=mesh['sp'=16,'tp'=2] {'sp'}, dimensions={0}, use_global_device_ids=true | all-gather | bytes 34816 | tf_op jit(solution)/shard_map/all_gather | solution.py:22
  139.6 15.4 %all-gather.16.cloned.1.call-done = f32[64,128,128]{2,1,0:T(8,128)} async-done(((f32[4,128,128]{2,1,0:T(8,128)}), f32[64,128,128]{2,1,0:T(8,128)}) %all-gather.16.cloned.1.call-update) | async-done | bytes 4194320 | tf_op jit(solution)/shard_map/all_gather | solution.py:22
  156.7 0.5 fusion.92
  161.0 3.7 convolution_convert_fusion.1
  164.8 6.0 tile.2
  170.8 38.8 %all-to-all-start = ((bf16[16,128,4096]{2,1,0:T(8,128)(2,1)}), bf16[16,128,4096]{2,1,0:T(8,128)(2,1)}, u32[]{:S(2)}, u32[]{:S(2)}) async-start(bf16[16,128,4096]{2,1,0:T(8,128)(2,1)} %tile.2), calls=%async_computation.1 | async-start | bytes 33554432 | tf_op jit(solution)/shard_map/all_to_all | solution.py:15
  209.6 0.5 all-gather.14.cloned.1.call-update
  210.2 1.1 fusion.39
  211.4 1.2 multiply_reduce_fusion.1
  212.6 1.1 multiply_convert_fusion.1
  213.7 2.4 all_gather.70
  216.0 367.9 %all-to-all-done = bf16[16,128,4096]{2,1,0:T(8,128)(2,1)} async-done(((bf16[16,128,4096]{2,1,0:T(8,128)(2,1)}), bf16[16,128,4096]{2,1,0:T(8,128)(2,1)}, u32[]{:S(2)}, u32[]{:S(2)}) %all-to-all-start) | async-done | bytes 16777248 | tf_op jit(solution)/shard_map/all_to_all | solution.py:15
  583.9 192.4 %all-gather.14.cloned.1.call-done = bf16[4096,2048]{1,0:T(8,128)(2,1)} async-done(((bf16[4096,128]{1,0:T(8,128)(2,1)}), bf16[4096,2048]{1,0:T(8,128)(2,1)}) %all-gather.14.cloned.1.call-update) | async-done | bytes 16777232 | tf_op jit(solution)/shard_map/all_gather | solution.py:182
  776.3 15.9 %convolution_convert_fusion = bf16[128,2048]{1,0:T(8,128)(2,1)} fusion(bf16[4096,2048]{1,0:T(8,128)(2,1)} %all-gather.14.cloned.1.call-done, bf16[128,2048]{1,0:T(8,128)(2,1)S(1)} %all_gather.70, bf16[2048,4096]{1,0:T(8,128)(2,1)} %bitcast.57), kind=kOutput, calls=%fused_computation.65 | convolution fusion | flops 4296802304 | bytes 34603008 | tf_op jit(solution)/shard_map/dot_general | solution.py:204
  792.2 23.5 %reduce-scatter.5.cloned.1.call-done = bf16[64,2048]{1,0:T(8,128)(2,1)} async-done(((bf16[128,2048]{1,0:T(8,128)(2,1)}), bf16[64,2048]{1,0:T(8,128)(2,1)}) %reduce-scatter.5.cloned.1.call-update) | async-done | bytes 262160 | tf_op jit(solution)/shard_map/reduce_scatter | solution.py:206
  815.6 1.1 fusion.41
  816.8 1.2 multiply_reduce_fusion
  818.0 1.8 multiply_convert_fusion
  (175 shorter events, 11.5 us)
Async XLA Ops:
  6.5 9.0 %copy-start.4 = (bf16[128,512]{1,0:T(8,128)(2,1)S(1)}, bf16[128,512]{1,0:T(8,128)(2,1)}, u32[]{:S(2)}) copy-start(bf16[128,512]{1,0:T(8,128)(2,1)} %param.22) | copy-start | bytes 393220
  6.5 133.0 %all-gather.18.cloned.1.call-start = ((), (), s32[]{:S(2)}) async-start(), calls=%async_computation.7 | async-start | bytes 2228224 | tf_op jit(solution)/shard_map/all_gather | solution.py:22
  13.4 0.6 copy-start.1
  14.0 140.9 %all-gather.16.cloned.1.call-start = ((), (), s32[]{:S(2)}) async-start(), calls=%async_computation.6 | async-start | bytes 4456448 | tf_op jit(solution)/shard_map/all_gather | solution.py:22
  16.2 2.4 copy-start.11
  16.2 48.6 %copy-start.5 = (bf16[128,512]{1,0:T(8,128)(2,1)S(1)}, bf16[128,512]{1,0:T(8,128)(2,1)}, u32[]{:S(2)}) copy-start(bf16[128,512]{1,0:T(8,128)(2,1)} %param.21) | copy-start | bytes 393220
  16.9 48.0 %copy-start.6 = (bf16[128,256]{1,0:T(8,128)(2,1)S(1)}, bf16[128,256]{1,0:T(8,128)(2,1)}, u32[]{:S(2)}) copy-start(bf16[128,256]{1,0:T(8,128)(2,1)} %param.23) | copy-start | bytes 196612
  17.7 0.7 copy-start
  18.4 191.8 %reduce-scatter.3.cloned.1.call-start = ((), (), s32[]{:S(2)}) async-start(), calls=%async_computation.3 | async-start | bytes 786432 | tf_op jit(solution)/shard_map/reduce_scatter | solution.py:184
  157.2 3.8 copy-start.9
  157.2 3.8 copy-start.10
  160.6 4.2 copy-start.3
  170.8 39.5 %copy-start.2 = (bf16[128,2048]{1,0:T(8,128)(2,1)S(1)}, bf16[128,2048]{1,0:T(8,128)(2,1)}, u32[]{:S(2)}) copy-start(bf16[128,2048]{1,0:T(8,128)(2,1)} %param.31) | copy-start | bytes 1572868
  170.8 41.8 %copy-start.7 = (f32[2048]{0:T(1024)S(1)}, f32[2048]{0:T(1024)}, u32[]{:S(2)}) copy-start(f32[2048]{0:T(1024)} %param.32) | copy-start | bytes 24580
  170.8 413.1 %all-to-all-start = ((bf16[16,128,4096]{2,1,0:T(8,128)(2,1)}), bf16[16,128,4096]{2,1,0:T(8,128)(2,1)}, u32[]{:S(2)}, u32[]{:S(2)}) async-start(bf16[16,128,4096]{2,1,0:T(8,128)(2,1)} %tile.2), calls=%async_computation.1 | async-start | bytes 33554432 | tf_op jit(solution)/shard_map/all_to_all | solution.py:15
  209.6 566.7 %all-gather.14.cloned.1.call-start = ((), (), s32[]{:S(2)}) async-start(), calls=%async_computation.4 | async-start | bytes 17825792 | tf_op jit(solution)/shard_map/all_gather | solution.py:182
  210.1 605.5 %reduce-scatter.5.cloned.1.call-start = ((), (), s32[]{:S(2)}) async-start(), calls=%async_computation.5 | async-start | bytes 786432 | tf_op jit(solution)/shard_map/reduce_scatter | solution.py:206
  776.3 41.7 %copy-start.8 = (f32[2048]{0:T(1024)S(1)}, f32[2048]{0:T(1024)}, u32[]{:S(2)}) copy-start(f32[2048]{0:T(1024)} %param.35) | copy-start | bytes 24580
Sparse Core Ops, SparseCore 0:
  14.2 63.5 all-gather.17
  80.5 74.4 all-gather.15
  164.9 40.8 reduce-scatter.2
  212.8 563.4 all-gather.13
  792.3 23.2 reduce-scatter.4
